TPU v7x, 32 devices: a whole 2x2x4 slice. The times are simulated.
32 devices in a mesh: sp: 16 (over z, y, x), tp: 2 (over core).
Axes of the slice: x: 2, y: 2, z: 4, core: 2. Of those that a mesh axis runs over, the one named last changes fastest.
Arguments:
- latent: bfloat16 [4096, 2048], P(('sp', 'tp')), may hold values from -6 to 6
- context: bfloat16 [512, 2048], P('sp'), may hold values from -6 to 6
- condition: float32 [2048], P('tp'), may hold values from -6 to 6
- context_condition: float32 [2048], P('tp'), may hold values from -6 to 6
- modulation_weight: bfloat16 [2048, 6144], P('tp', 'sp'), may hold values from -0.125 to 0.125
- query_first: bfloat16 [2048, 512], P(None, 'tp'), may hold values from -1 to 1
- query_second: bfloat16 [2048, 512], P(None, 'tp'), may hold values from -1 to 1
- key_first: bfloat16 [2048, 512], P(None, 'tp'), may hold values from -1 to 1
- key_second: bfloat16 [2048, 512], P(None, 'tp'), may hold values from -1 to 1
- value_weight: bfloat16 [2048, 1024], P(None, 'tp'), may hold values from -0.125 to 0.125
- lambda_head: float32 [8], P('tp'), may hold values from 0.3 to 0.8
- context_score_boost: float32 [8], P('tp'), may hold values from 1.5 to 3
- head_gain: float32 [128], replicated, may hold values from 0.1 to 1.9
- output_weight: bfloat16 [1024, 2048], P('tp'), may hold values from -0.1875 to 0.1875
Outputs:
- updated: bfloat16 [4096, 2048], P(('sp', 'tp'))
All inputs are finite; a program needn't handle non-finite values.
Results may differ from a plain program's by a relative error of at most 0.0095.
Values may be sent and summed in bfloat16 or wider, within the bound.
A program may use at most 64 MiB of HBM per device.

v0:
```python
import jax
import jax.numpy as jnp
from jax import lax
from jax.sharding import PartitionSpec as P

HEAD_DIM = 64
VALUE_DIM = 128
GRID_W = 64


EPSILON = 1e-06
THETA = 10000.0
NEGATIVE = -1e30


def norm_rows(rows):
    values = rows.astype(jnp.float32)
    return values * lax.rsqrt(jnp.mean(values * values, axis=-1, keepdims=True) + EPSILON)


def rotate_pairs(values, positions):
    half = values.shape[-1] // 2
    quarter = half // 2
    reciprocal_norm = THETA ** (-jnp.arange(quarter, dtype=jnp.float32) / quarter)

    def turn(part, where):
        angle = where.astype(jnp.float32)[:, None] * reciprocal_norm[None, :]
        cosine_table = jnp.concatenate([jnp.cos(angle)] * 2, -1)[:, None, :]
        sine = jnp.concatenate([jnp.sin(angle)] * 2, -1)[:, None, :]
        flipped = jnp.concatenate([-part[..., quarter:], part[..., :quarter]], -1)
        return part * cosine_table + flipped * sine

    grid_row = positions // GRID_W
    grid_col = positions % GRID_W
    return jnp.concatenate(
        [turn(values[..., :half], grid_row), turn(values[..., half:], grid_col)], -1
    )


def block_extent(rows):
    size = min(rows, 1024)
    while rows % size:
        size -= 1
    return size


def body(
    latent,
    context,
    condition,
    context_condition,
    modulation_weight,
    query_first,
    query_second,
    key_first,
    key_second,
    value_weight,
    lambda_head,
    context_score_boost,
    head_gain,
    output_weight,
):
    width = latent.shape[1]
    signal = jax.nn.silu(jnp.stack([condition, context_condition])).astype(jnp.bfloat16)
    partial_mod = jnp.dot(signal, modulation_weight, preferred_element_type=jnp.float32)
    reduced = lax.psum(partial_mod, "tp")
    modulation = lax.all_gather(reduced, "sp", axis=1, tiled=True)
    shift = modulation[:, :width]
    scale = modulation[:, width : 2 * width]
    gate = modulation[:, 2 * width :]
    h_latent = (norm_rows(latent) * (1.0 + scale[0]) + shift[0]).astype(jnp.bfloat16)
    h_context = (norm_rows(context) * (1.0 + scale[1]) + shift[1]).astype(jnp.bfloat16)
    heads_dev = value_weight.shape[1] // VALUE_DIM
    span = heads_dev * HEAD_DIM
    offset = lax.axis_index("sp") * (latent.shape[0] * lax.axis_size("tp"))
    piece = lax.all_gather(h_latent, "tp", axis=0, tiled=True)
    count = piece.shape[0]
    positions = offset + jnp.arange(count, dtype=jnp.int32)
    turned = []
    for weight in (query_first, query_second, key_first, key_second):
        product = jnp.dot(piece, weight, preferred_element_type=jnp.float32).reshape(
            count, heads_dev, HEAD_DIM
        )
        turned.append(rotate_pairs(product, positions).astype(jnp.bfloat16).reshape(count, span))
    values = jnp.dot(piece, value_weight, preferred_element_type=jnp.float32).astype(jnp.bfloat16)
    projected = jnp.concatenate(turned + [values], axis=1)
    queries = projected.shape[0]
    queries_one = projected[:, :span].reshape(queries, heads_dev, HEAD_DIM)
    queries_two = projected[:, span : 2 * span].reshape(queries, heads_dev, HEAD_DIM)
    latent_keys = projected[:, 2 * span : 4 * span]
    latent_values = projected[:, 4 * span :]

    def update(carry, block):
        keys_pair, values, boolean_markers = block
        count = keys_pair.shape[0]
        keys_one = keys_pair[:, :span].reshape(count, heads_dev, HEAD_DIM)
        keys_two = keys_pair[:, span:].reshape(count, heads_dev, HEAD_DIM)
        values_heads = values.reshape(count, heads_dev, VALUE_DIM)
        extra_score = context_score_boost[:, None, None] * boolean_markers[None, None, :]
        renewed = []
        for (highest, totals, weighted), query, keys in zip(
            carry, (queries_one, queries_two), (keys_one, keys_two)
        ):
            scores = (
                jnp.einsum("qhd,khd->hqk", query, keys, preferred_element_type=jnp.float32)
                * HEAD_DIM ** (-0.5)
                + extra_score
            )
            peak = jnp.maximum(highest, jnp.max(scores, axis=-1))
            exp_weights = jnp.exp(scores - peak[..., None])
            rescale = jnp.exp(highest - peak)
            totals = totals * rescale + jnp.sum(exp_weights, axis=-1)
            weighted = weighted * jnp.transpose(rescale)[:, :, None] + jnp.einsum(
                "hqk,khe->qhe",
                exp_weights.astype(jnp.bfloat16),
                values_heads,
                preferred_element_type=jnp.float32,
            )
            renewed.append((peak, totals, weighted))
        return (tuple(renewed), None)

    def fold_keys(carry, keys_pair, values, boolean_markers):
        rows = keys_pair.shape[0]
        size = block_extent(rows)
        count = rows // size
        blocks = (
            keys_pair.reshape(count, size, keys_pair.shape[1]),
            values.reshape(count, size, values.shape[1]),
            boolean_markers.reshape(count, size),
        )
        carry, unused = lax.scan(update, carry, blocks)
        return carry

    start_state = (
        jnp.full((heads_dev, queries), NEGATIVE, jnp.float32),
        jnp.zeros((heads_dev, queries), jnp.float32),
        jnp.zeros((queries, heads_dev, VALUE_DIM), jnp.float32),
    )
    initial = (start_state, start_state)
    keys_pair = jnp.concatenate(
        [
            jnp.dot(h_context, key_first, preferred_element_type=jnp.float32).astype(jnp.bfloat16),
            jnp.dot(h_context, key_second, preferred_element_type=jnp.float32).astype(jnp.bfloat16),
        ],
        axis=1,
    )
    values = jnp.dot(h_context, value_weight, preferred_element_type=jnp.float32).astype(
        jnp.bfloat16
    )
    all_keys, all_values = (
        lax.all_gather(keys_pair, "sp", axis=0, tiled=True),
        lax.all_gather(values, "sp", axis=0, tiled=True),
    )
    carry = fold_keys(initial, all_keys, all_values, jnp.ones((all_keys.shape[0],), jnp.float32))
    pieces = (
        lax.all_gather(latent_keys, "sp", axis=0, tiled=True),
        lax.all_gather(latent_values, "sp", axis=0, tiled=True),
    )
    boolean_markers = jnp.zeros((pieces[0].shape[0],), jnp.float32)
    final = fold_keys(carry, pieces[0], pieces[1], boolean_markers)
    outcomes = [weighted / jnp.transpose(totals)[:, :, None] for highest, totals, weighted in final]
    mixed = outcomes[0] - lambda_head[None, :, None] * outcomes[1]
    normed = (
        mixed * lax.rsqrt(jnp.mean(mixed * mixed, axis=-1, keepdims=True) + EPSILON) * head_gain
    )
    heads_out = normed.astype(jnp.bfloat16).reshape(queries, heads_dev * VALUE_DIM)
    branch = lax.psum_scatter(
        jnp.dot(heads_out, output_weight, preferred_element_type=jnp.float32).astype(jnp.bfloat16),
        "tp",
        scatter_dimension=0,
        tiled=True,
    ).astype(jnp.float32)
    return (latent.astype(jnp.float32) + gate[0] * branch).astype(jnp.bfloat16)


def solution(mesh):
    in_specs = (
        P(("sp", "tp"), None),
        P("sp", None),
        P("tp"),
        P("tp"),
        P("tp", "sp"),
        P(None, "tp"),
        P(None, "tp"),
        P(None, "tp"),
        P(None, "tp"),
        P(None, "tp"),
        P("tp"),
        P("tp"),
        P(),
        P("tp", None),
    )
    out_specs = P(("sp", "tp"), None)
    return jax.shard_map(body, mesh=mesh, in_specs=in_specs, out_specs=out_specs, check_vma=False)
```

profile of v0, /device:TPU:0, one launch (start us, length us, event | category | flops | bytes accessed | tf_op | source)
XLA Modules:
  0.0 315.9 jit_solution(17593726352576110666)
XLA Ops:
  6.5 1.4 fusion.40
  7.9 1.3 fusion.74
  9.3 2.6 psum.7
  11.9 42.5 %all_gather.18 = f32[2,6144]{1,0:T(2,128)S(1)} all-gather(f32[2,384]{1,0:T(2,128)S(1)} %psum.7), channel_id=1, replica_groups=mesh['sp'=16,'tp'=2] {'sp'}, dimensions={1}, use_global_device_ids=true | all-gather | bytes 52224 | tf_op jit(solution)/shard_map/all_gather | solution.py:67
  55.0 2.1 fusion.43
  57.2 5.0 %all-gather.4.cloned.1.call-done = bf16[256,2048]{1,0:T(8,128)(2,1)} async-done(((bf16[128,2048]{1,0:T(8,128)(2,1)}), bf16[256,2048]{1,0:T(8,128)(2,1)}) %all-gather.4.cloned.1.call-update) | async-done | bytes 1048592 | tf_op jit(solution)/shard_map/all_gather | solution.py:76
  62.2 3.4 %convolution_convert_fusion.1 = bf16[256,512]{1,0:T(8,128)(2,1)} fusion(bf16[256,2048]{1,0:T(8,128)(2,1)} %all-gather.4.cloned.1.call-done, bf16[2048,512]{1,0:T(8,128)(2,1)} %param.25), kind=kOutput, calls=%fused_computation.53 | convolution fusion | flops 537001984 | bytes 3407872 | tf_op jit(solution)/shard_map/dot_general | solution.py:85
  66.0 1.8 fusion.99
  68.7 1.8 fusion.100
  73.2 2.1 convolution_convert_fusion.2
  75.3 45.0 %all_gather.21 = bf16[512,512]{1,0:T(8,128)(2,1)S(1)} all-gather(bf16[32,512]{1,0:T(8,128)(2,1)S(1)} %convolution_convert_fusion.2), channel_id=1, replica_groups=mesh['sp'=16,'tp'=2] {'sp'}, dimensions={0}, use_global_device_ids=true | all-gather | bytes 557056 | tf_op jit(solution)/shard_map/all_gather | solution.py:152
  120.5 1.6 convolution_convert_fusion.3
  122.1 1.6 convolution_convert_fusion.4
  123.7 42.0 %all_gather.20 = bf16[512,512]{1,0:T(8,128)(2,1)S(1)} all-gather(bf16[32,512]{1,0:T(8,128)(2,1)S(1)} %pad_maximum_fusion.9), channel_id=1, replica_groups=mesh['sp'=16,'tp'=2] {'sp'}, dimensions={0}, use_global_device_ids=true | all-gather | bytes 557056 | tf_op jit(solution)/shard_map/all_gather | solution.py:151
  166.9 1.4 fusion.89
  170.2 1.5 fusion.38
  171.7 1.5 fusion.39
  173.2 56.5 %all-gather.6.cloned.1.call-done = bf16[4096,512]{1,0:T(8,128)(2,1)} async-done(((bf16[256,512]{1,0:T(8,128)(2,1)}), bf16[4096,512]{1,0:T(8,128)(2,1)}) %all-gather.6.cloned.1.call-update) | async-done | bytes 4194320 | tf_op jit(solution)/shard_map/all_gather | solution.py:156
  229.7 67.3 %while.2 = (s32[]{:T(128)}, f32[4,256]{1,0:T(4,128)S(1)}, f32[4,256]{1,0:T(4,128)S(1)}, f32[256,4,128]{0,2,1:T(8,128)}, f32[4,256]{1,0:T(4,128)S(1)}, /*index=5*...) while((s32[]{:T(128)}, f32[4,256]{1,0:T(4,128)S(1)}, ...), condition=%wide.region_12.13_spmd, body=%wide.region_7.12_spmd.sunk | while | flops 828905472 | bytes 53870940 | solution.py:131
  229.7 2.4 constant_dynamic-slice_fusion.5
  232.1 1.5 copy.40
  233.6 2.4 constant_dynamic-slice_fusion.4
  235.9 2.3 copy.39
  238.2 1.3 fusion.150
  240.3 1.4 bitcast_reduce_fusion.3
  241.7 1.7 fusion.154
  246.5 2.4 constant_dynamic-slice_fusion.5
  248.9 1.5 copy.40
  250.4 2.4 constant_dynamic-slice_fusion.4
  252.7 2.3 copy.39
  257.1 1.4 bitcast_reduce_fusion.3
  258.5 1.7 fusion.154
  263.4 2.4 constant_dynamic-slice_fusion.5
  265.7 1.5 copy.40
  267.2 2.4 constant_dynamic-slice_fusion.4
  269.6 2.3 copy.39
  273.9 1.4 bitcast_reduce_fusion.3
  275.3 1.7 fusion.154
  280.2 2.4 constant_dynamic-slice_fusion.5
  282.5 1.5 copy.40
  284.0 2.4 constant_dynamic-slice_fusion.4
  286.4 2.3 copy.39
  290.7 1.4 bitcast_reduce_fusion.3
  292.1 1.7 fusion.154
  297.0 1.4 multiply_reduce_fusion
  298.5 1.7 convolution_convert_fusion
  300.2 7.2 %reduce-scatter.2.cloned.1.call-done = bf16[128,2048]{1,0:T(8,128)(2,1)} async-done(((bf16[256,2048]{1,0:T(8,128)(2,1)}), bf16[128,2048]{1,0:T(8,128)(2,1)}) %reduce-scatter.2.cloned.1.call-update) | async-done | bytes 524304 | tf_op jit(solution)/shard_map/reduce_scatter | solution.py:167
  307.4 2.0 fusion.44
  (153 shorter events, 27.1 us)
Async XLA Ops:
  6.5 291.9 %copy-start = (bf16[512,2048]{1,0:T(8,128)(2,1)S(1)}, bf16[512,2048]{1,0:T(8,128)(2,1)}, u32[]{:S(2)}) copy-start(bf16[512,2048]{1,0:T(8,128)(2,1)} %param.29) | copy-start | bytes 6291460
  6.5 55.6 %all-gather.4.cloned.1.call-start = ((), (), s32[]{:S(2)}) async-start(), calls=%async_computation.1 | async-start | bytes 1572864 | tf_op jit(solution)/shard_map/all_gather | solution.py:76
  57.1 116.1 %all-gather.8.cloned.1.call-start = ((), (), s32[]{:S(2)}) async-start(), calls=%async_computation.3 | async-start | bytes 4456448 | tf_op jit(solution)/shard_map/all_gather | solution.py:157
  62.2 3.8 %copy-start.5 = (bf16[256,2048]{1,0:T(8,128)(2,1)S(1)}, bf16[256,2048]{1,0:T(8,128)(2,1)}, u32[]{:S(2)}) copy-start(bf16[256,2048]{1,0:T(8,128)(2,1)} %all-gather.4.cloned.1.call-done) | copy-start | bytes 3145732
  65.6 164.1 %all-gather.6.cloned.1.call-start = ((), (), s32[]{:S(2)}) async-start(), calls=%async_computation.2 | async-start | bytes 4456448 | tf_op jit(solution)/shard_map/all_gather | solution.py:156
  65.6 2.1 copy-start.8
  65.9 2.5 copy-start.10
  65.9 2.5 copy-start.12
  66.0 2.5 copy-start.14
  66.0 2.4 copy-start.16
  68.7 1.9 copy-start.9
  70.5 0.8 copy-start.11
  70.5 0.8 copy-start.13
  70.6 0.8 copy-start.15
  70.6 0.8 copy-start.17
  71.1 1.9 copy-start.7
  73.0 234.4 %reduce-scatter.2.cloned.1.call-start = ((), (), s32[]{:S(2)}) async-start(), calls=%async_computation.4 | async-start | bytes 1572864 | tf_op jit(solution)/shard_map/reduce_scatter | solution.py:167
  165.7 2.6 copy-start.19
  229.7 67.3 %copy-start.20 = (f32[4]{0:T(128)S(1)}, f32[4]{0:T(128)}, u32[]{:S(2)}) copy-start(f32[4]{0:T(128)} %param.26) | copy-start | bytes 52
  229.7 68.7 %copy-start.21 = (f32[128]{0:T(128)S(1)}, f32[128]{0:T(128)}, u32[]{:S(2)}) copy-start(f32[128]{0:T(128)} %param.28) | copy-start | bytes 1540
  241.7 1.7 copy-start.3
  243.4 1.2 copy-start.1
  244.6 1.2 copy-start.4
  245.7 0.8 copy-start.2
  258.5 1.7 copy-start.3
  260.2 1.2 copy-start.1
  261.4 1.2 copy-start.4
  262.5 0.8 copy-start.2
  275.3 1.7 copy-start.3
  277.0 1.2 copy-start.1
  278.2 1.2 copy-start.4
  279.4 0.8 copy-start.2
  292.1 1.7 copy-start.3
  293.8 1.2 copy-start.1
  295.0 1.2 copy-start.4
  296.2 0.8 copy-start.2
  298.5 8.9 %copy-start.6 = (bf16[128,2048]{1,0:T(8,128)(2,1)S(1)}, bf16[128,2048]{1,0:T(8,128)(2,1)}, u32[]{:S(2)}) copy-start(bf16[128,2048]{1,0:T(8,128)(2,1)} %param.16) | copy-start | bytes 1572868
  298.5 8.9 %copy-start.18 = (f32[1,2048]{1,0:T(1,128)S(1)}, f32[1,2048]{1,0:T(1,128)}, u32[]{:S(2)}) copy-start(f32[1,2048]{1,0:T(1,128)} %get-tuple-element.207) | copy-start | bytes 24580
Sparse Core Ops, SparseCore 0:
  57.2 4.8 all-gather.3
  65.7 86.1 all-gather.7
  154.7 74.9 all-gather.5
  300.4 6.9 reduce-scatter.1
where the time goes:
time: 317 us; the launch traced here: 316 us
  blocking collectives  132 us (42%)
  waiting for transfers between devices  68.7 us (22%)
  local copies, waits for them, and re-layouts  43 us (14%)
  matrix products  39.2 us (12%)
  other arithmetic  18.8 us (6%)
  between operations  13.6 us (4%)
    all_gather x1, waiting for transfers between devices, body(): lax.all_gather(latent_keys, 'sp', axis=0, tiled=True)  56.5 us
    all_gather x1, blocking collectives, body(): lax.all_gather(values, 'sp', axis=0, tiled=True)  45 us
    all_gather x1, blocking collectives, body(): modulation = lax.all_gather(reduced, 'sp', axis=1, tiled=True)  42.5 us
    all_gather x1, blocking collectives, body(): lax.all_gather(keys_pair, 'sp', axis=0, tiled=True)  42 us
    dynamic_slice x16, local copies, waits for them, and re-layouts, fold_keys(): carry, unused = lax.scan(update, carry, blocks)  33.9 us
    dot_general x10, matrix products, update(): jnp.einsum('hqk,khe->qhe', exp_weights.astype(jnp.bfloat16), values_heads...  12.1 us
    dot_general x10, matrix products, update(): jnp.einsum('qhd,khd->hqk', query, keys, preferred_element_type=jnp.float32)  10.6 us
    reduce_sum x5, other arithmetic, update(): totals = totals * rescale + jnp.sum(exp_weights, axis=-1)  8.09 us
  transfers between devices with their start and end apart: 4, of which 3 were waited for; matrix products, arithmetic and copies ran while one was open for 6% of the time, Pallas kernels for 0%

commit v1 on v0

v1 whole, which is shorter than its diff:
```python
import functools
import math

import jax
import jax.numpy as jnp
from jax import lax
from jax.experimental import pallas as pl
from jax.experimental.pallas import tpu as pltpu
from jax.sharding import PartitionSpec as P

HEAD_DIM = 64
VALUE_DIM = 128
GRID_W = 64
EPSILON = 1e-06
THETA = 10000.0
NEGATIVE = -1e30
LOG2E = math.log2(math.e)
MESH = pl.DeviceIdType.MESH
BF16 = jnp.bfloat16
F32 = jnp.float32
LANES = 128


def rotation_tables(positions, extra):
    half = HEAD_DIM // 2
    quarter = half // 2
    rates = THETA ** (-jnp.arange(quarter, dtype=F32) / quarter)
    lane = jnp.arange(LANES) % HEAD_DIM
    rate = rates[lane % quarter]
    where = jnp.where(
        (lane < half)[None, :], (positions // GRID_W)[:, None], (positions % GRID_W)[:, None]
    ).astype(F32)
    angle = where * rate[None, :]
    sign = jnp.where(lane % half < quarter, -1.0, 1.0).astype(F32)
    cosine = jnp.concatenate([jnp.cos(angle), jnp.ones((extra, LANES), F32)], 0)
    sine = jnp.concatenate([jnp.sin(angle) * sign[None, :], jnp.zeros((extra, LANES), F32)], 0)
    return cosine, sine


def rotate(x, cosine, sine):
    quarter = HEAD_DIM // 4
    lane = lax.broadcasted_iota(jnp.int32, x.shape, 1)
    ahead = pltpu.roll(x, LANES - quarter, 1)
    behind = pltpu.roll(x, quarter, 1)
    flipped = jnp.where(lane % (2 * quarter) < quarter, ahead, behind)
    return x * cosine + flipped * sine


def normed_rows(rows, scale, shift):
    v = rows.astype(F32)
    v = v * lax.rsqrt(jnp.mean(v * v, axis=-1, keepdims=True) + EPSILON)
    return (v * (1.0 + scale) + shift).astype(BF16)


def kernel(
    dims,
    latent_ref, context_ref, cond_ref, ccond_ref, modw_ref,
    wq1_hbm, wq2_hbm, wk1_hbm, wk2_hbm, wv_hbm,
    lam_ref, boost_ref, gain_ref, wo_hbm, cos_ref, sin_ref,
    out_ref,
    wq1, wq2, wk1, wk2, wv, wo,
    sig, modp, modall, modrow, lat, h,
    qs, kvs, q, kv, mx, den, acc, ho, hr, rsend, rs,
    wsem, mp_s, mp_r, lt_s, lt_r, ma_s, ma_r,
    q_s, q_r, kz_s, kv_s, kv_r, ho_s, ho_r, rs_s, rs_r,
):
    S, T, G, R, B, Cr, cw = dims
    s, t = lax.axis_index("sp"), lax.axis_index("tp")
    g, r = s // R, s % R
    rows, D = latent_ref.shape
    Lr = rows * T
    Cp = context_ref.shape[0]

    def remote(src, dst, send, recv, sp, tp):
        return pltpu.make_async_remote_copy(
            src_ref=src, dst_ref=dst, send_sem=send, recv_sem=recv,
            device_id=(sp, tp), device_id_type=MESH,
        )

    loads = [
        pltpu.make_async_copy(a, b, wsem.at[i])
        for i, (a, b) in enumerate(
            [(wk1_hbm, wk1), (wk2_hbm, wk2), (wv_hbm, wv), (wq1_hbm, wq1), (wq2_hbm, wq2), (wo_hbm, wo)]
        )
    ]
    for load in loads:
        load.start()

    barrier = pltpu.get_barrier_semaphore()

    @pl.loop(1, S)
    def _(i):
        pl.semaphore_signal(barrier, inc=1, device_id=((s + i) % S, t), device_id_type=MESH)

    for i in range(1, T):
        pl.semaphore_signal(barrier, inc=1, device_id=(s, (t + i) % T), device_id_type=MESH)

    for i, ref in enumerate((cond_ref, ccond_ref)):
        v = ref[...]
        sig[i : i + 1, :] = v / (1.0 + jnp.exp(-v))
    modp[t] = jnp.dot(sig[...].astype(BF16), modw_ref[...], preferred_element_type=F32)

    pl.semaphore_wait(barrier, S - 1 + T - 1)

    def part_copy(i):
        return remote(modp.at[t], modp.at[t], mp_s.at[i], mp_r.at[t], s, (t + i) % T)

    def latent_copy(i):
        return remote(latent_ref, lat.at[t], lt_s.at[i], lt_r.at[t], s, (t + i) % T)

    for i in range(1, T):
        part_copy(i).start()
    for i in range(1, T):
        latent_copy(i).start()
    lat[t] = latent_ref[...]
    for i in range(1, T):
        o = (t + i) % T
        remote(modp.at[o], modp.at[o], mp_s.at[i], mp_r.at[o], s, o).wait_recv()
    total = modp[0]
    for i in range(1, T):
        total = total + modp[i]
    modall[s] = total

    def mod_copy(i, src):
        return remote(modall.at[src], modall.at[src], ma_s.at[i], ma_r.at[src], (s + i) % S, t)

    @pl.loop(1, S)
    def _(i):
        mod_copy(i, s).start()

    for i in range(1, T):
        o = (t + i) % T
        remote(lat.at[o], lat.at[o], lt_s.at[i], lt_r.at[o], s, o).wait_recv()

    @pl.loop(1, S)
    def _(i):
        mod_copy(i, (s + i) % S).wait_recv()

    for i in range(S):
        modrow[:, i * cw : (i + 1) * cw] = modall[i][:, :cw]

    step = math.gcd(rows, 32)
    for i in range(T):

        @pl.loop(0, rows // step)
        def _(j):
            at = pl.multiple_of(j * step, step)
            h[pl.ds(i * rows + at, step), :] = normed_rows(
                lat[i, pl.ds(at, step), :], modrow[0:1, D : 2 * D], modrow[0:1, :D]
            )

    h[Lr:, :] = normed_rows(context_ref[...], modrow[1:2, D : 2 * D], modrow[1:2, :D])

    for i in range(3):
        loads[i].wait()
    hh = h[...]
    one = jnp.dot(hh, wk1[...], preferred_element_type=F32)
    two = jnp.dot(hh, wk2[...], preferred_element_type=F32)
    for i in range(G):
        cut = slice(i * HEAD_DIM, (i + 1) * HEAD_DIM)
        pair = jnp.concatenate([one[:, cut], two[:, cut]], axis=1)
        kvs[i, :, :LANES] = rotate(pair, cos_ref[...], sin_ref[...]).astype(BF16)
    val = jnp.dot(hh, wv[...], preferred_element_type=F32)
    for i in range(G):
        kvs[i, :, LANES:] = val[:, i * VALUE_DIM : (i + 1) * VALUE_DIM].astype(BF16)

    def kv_out(i):
        to = (g + i) % G
        return remote(kvs.at[to], kv.at[s], kz_s.at[i], kv_r.at[s], to * R + r, t)

    for i in range(1, G):
        kv_out(i).start()
    kv[s] = kvs[g]

    def forward(i, j):
        src = ((g + G - i) % G) * R + r
        return remote(kv.at[src], kv.at[src], kv_s.at[i, j], kv_r.at[src], g * R + (r + j) % R, t)

    def landed(src):
        remote(kv.at[src], kv.at[src], kz_s.at[0], kv_r.at[src], s, t).wait_recv()

    def forward_all(i):
        @pl.loop(1, R)
        def _(j):
            forward(i, j).start()

    forward_all(0)
    for i in range(3, 5):
        loads[i].wait()
    lh = h[:Lr, :]
    one = jnp.dot(lh, wq1[...], preferred_element_type=F32)
    two = jnp.dot(lh, wq2[...], preferred_element_type=F32)
    for i in range(G):
        cut = slice(i * HEAD_DIM, (i + 1) * HEAD_DIM)
        pair = jnp.concatenate([one[:, cut], two[:, cut]], axis=1)
        turned = rotate(pair, cos_ref[:Lr, :], sin_ref[:Lr, :])
        qs[i] = (turned * (LOG2E * HEAD_DIM**-0.5)).astype(BF16)

    def q_out(i):
        to = (g + i) % G
        return remote(qs.at[to], q.at[g], q_s.at[i], q_r.at[g], to * R + r, t)

    for i in range(1, G):
        q_out(i).start()
    q[g] = qs[g]

    mx[...] = jnp.full(mx.shape, NEGATIVE, F32)
    den[...] = jnp.zeros(den.shape, F32)
    acc[...] = jnp.zeros(acc.shape, F32)
    boost = boost_ref[g] * LOG2E

    for i in range(1, G):
        o = (g + i) % G
        remote(q.at[o], q.at[o], q_s.at[i], q_r.at[o], s, t).wait_recv()

    for i in range(G):
        if i + 1 < G:
            landed(((g + G - i - 1) % G) * R + r)
            forward_all(i + 1)
        base = ((g + G - i) % G) * R

        @pl.loop(1, R)
        def _(j):
            landed(base + (r + j) % R)

        @pl.loop(0, (R // B) * G)
        def _(n):
            at = base + (n // G) * B
            n = n % G
            k_l = kv[pl.ds(at, B), :Lr, :LANES].reshape(B * Lr, LANES)
            v_l = kv[pl.ds(at, B), :Lr, LANES:].reshape(B * Lr, VALUE_DIM)
            k_c = kv[pl.ds(at, B), Lr:, :LANES].reshape(B * Cp, LANES)
            v_c = kv[pl.ds(at, B), Lr:, LANES:].reshape(B * Cp, VALUE_DIM)
            qq = q[n]
            lane = lax.broadcasted_iota(jnp.int32, qq.shape, 1)
            nt = (((1,), (1,)), ((), ()))
            for m in range(2):
                qm = jnp.where(lane // HEAD_DIM == m, qq, jnp.zeros_like(qq))
                s_l = lax.dot_general(qm, k_l, nt, preferred_element_type=F32)
                s_c = lax.dot_general(qm, k_c, nt, preferred_element_type=F32) + boost
                if Cp != Cr:
                    spot = lax.broadcasted_iota(jnp.int32, s_c.shape, 1)
                    s_c = jnp.where(spot % Cp < Cr, s_c, NEGATIVE)
                old = mx[m, n]
                peak = jnp.maximum(
                    old,
                    jnp.maximum(
                        jnp.max(s_l, axis=-1, keepdims=True), jnp.max(s_c, axis=-1, keepdims=True)
                    ),
                )
                p_l = jnp.exp2(s_l - peak)
                p_c = jnp.exp2(s_c - peak)
                alpha = jnp.exp2(old - peak)
                mx[m, n] = peak
                den[m, n] = (
                    alpha * den[m, n]
                    + jnp.sum(p_l, axis=-1, keepdims=True)
                    + jnp.sum(p_c, axis=-1, keepdims=True)
                )
                acc[m, n] = (
                    alpha * acc[m, n]
                    + jnp.dot(p_l.astype(BF16), v_l, preferred_element_type=F32)
                    + jnp.dot(p_c.astype(BF16), v_c, preferred_element_type=F32)
                )

    lam = lam_ref[g]
    gain = gain_ref[...]

    def ho_out(i):
        to = (g + i) % G
        return remote(ho.at[to], hr.at[g], ho_s.at[i], ho_r.at[g], to * R + r, t)

    for i in range(1, G + 1):
        n = (g + i) % G
        mixed = acc[0, n] / den[0, n] - lam * (acc[1, n] / den[1, n])
        mixed = mixed * lax.rsqrt(jnp.mean(mixed * mixed, axis=-1, keepdims=True) + EPSILON) * gain
        if i < G:
            ho[n] = mixed.astype(BF16)
            ho_out(i).start()
        else:
            hr[g] = mixed.astype(BF16)
    loads[5].wait()
    for i in range(1, G):
        o = (g + i) % G
        remote(hr.at[o], hr.at[o], ho_s.at[i], ho_r.at[o], s, t).wait_recv()

    def branch_rows(o):
        at = pl.multiple_of(o * rows, rows)
        mine = jnp.concatenate([hr[i, pl.ds(at, rows), :] for i in range(G)], axis=1)
        return jnp.dot(mine, wo[...], preferred_element_type=F32)

    def rs_out(i):
        o = (t + i) % T
        return remote(rsend.at[o], rs.at[t], rs_s.at[i], rs_r.at[t], s, o)

    for i in range(1, T):
        o = (t + i) % T
        rsend[o] = branch_rows(o).astype(BF16)
        rs_out(i).start()
    branch = branch_rows(t)
    for i in range(1, T):
        o = (t + i) % T
        remote(rs.at[o], rs.at[o], rs_s.at[i], rs_r.at[o], s, o).wait_recv()
        branch = branch + rs[o].astype(F32)
    out_ref[...] = (latent_ref[...].astype(F32) + modrow[0:1, 2 * D :] * branch).astype(BF16)

    for i in range(1, T):
        part_copy(i).wait_send()
        latent_copy(i).wait_send()
        rs_out(i).wait_send()

    @pl.loop(1, S)
    def _(i):
        mod_copy(i, s).wait_send()

    for i in range(1, G):
        kv_out(i).wait_send()
        q_out(i).wait_send()
        ho_out(i).wait_send()
    for i in range(G):

        @pl.loop(1, R)
        def _(j):
            forward(i, j).wait_send()


def body(
    S, T,
    latent, context, condition, context_condition, modulation_weight,
    query_first, query_second, key_first, key_second, value_weight,
    lambda_head, context_score_boost, head_gain, output_weight,
):
    rows, D = latent.shape
    Lr = rows * T
    G = value_weight.shape[1] // VALUE_DIM
    assert S % G == 0
    R = S // G
    B = math.gcd(R, 4)
    Cr = context.shape[0]
    Cp = -(-Cr // 16) * 16
    if Cp != Cr:
        context = jnp.pad(context, ((0, Cp - Cr), (0, 0)))
    cw = modulation_weight.shape[1]
    cp = -(-cw // LANES) * LANES
    if cp != cw:
        modulation_weight = jnp.pad(modulation_weight, ((0, 0), (0, cp - cw)))
    depth = modulation_weight.shape[0]
    positions = lax.axis_index("sp") * Lr + jnp.arange(Lr, dtype=jnp.int32)
    cosine, sine = rotation_tables(positions, Cp)
    vm = pl.BlockSpec(memory_space=pltpu.VMEM)
    sm = pl.BlockSpec(memory_space=pltpu.SMEM)
    hb = pl.BlockSpec(memory_space=pl.ANY)
    V = pltpu.VMEM
    dma = pltpu.SemaphoreType.DMA
    weights = (query_first, query_second, key_first, key_second, value_weight, output_weight)
    return pl.pallas_call(
        functools.partial(kernel, (S, T, G, R, B, Cr, cw)),
        out_shape=jax.ShapeDtypeStruct((rows, D), BF16),
        in_specs=[vm] * 5 + [hb] * 5 + [sm, sm, vm, hb, vm, vm],
        out_specs=vm,
        scratch_shapes=[V(w.shape, BF16) for w in weights]
        + [
            V((2, depth), F32),
            V((T, 2, cp), F32),
            V((S, 2, cp), F32),
            V((2, 3 * D), F32),
            V((T, rows, D), BF16),
            V((Lr + Cp, D), BF16),
            V((G, Lr, LANES), BF16),
            V((G, Lr + Cp, LANES + VALUE_DIM), BF16),
            V((G, Lr, LANES), BF16),
            V((S, Lr + Cp, LANES + VALUE_DIM), BF16),
            V((2, G, Lr, 1), F32),
            V((2, G, Lr, 1), F32),
            V((2, G, Lr, VALUE_DIM), F32),
            V((G, Lr, VALUE_DIM), BF16),
            V((G, Lr, VALUE_DIM), BF16),
            V((T, rows, D), BF16),
            V((T, rows, D), BF16),
            dma((6,)),
            dma((T,)), dma((T,)), dma((T,)), dma((T,)), dma((S,)), dma((S,)),
            dma((G,)), dma((G,)), dma((G,)), dma((G, R)), dma((S,)),
            dma((G,)), dma((G,)), dma((T,)), dma((T,)),
        ],
        compiler_params=pltpu.CompilerParams(
            collective_id=0, has_side_effects=True, vmem_limit_bytes=62 * 1024 * 1024
        ),
    )(
        latent, context, condition[None, :], context_condition[None, :], modulation_weight,
        query_first, query_second, key_first, key_second, value_weight,
        lambda_head, context_score_boost, head_gain[None, :], output_weight, cosine, sine,
    )


def solution(mesh):
    in_specs = (
        P(("sp", "tp"), None),
        P("sp", None),
        P("tp"),
        P("tp"),
        P("tp", "sp"),
        P(None, "tp"),
        P(None, "tp"),
        P(None, "tp"),
        P(None, "tp"),
        P(None, "tp"),
        P("tp"),
        P("tp"),
        P(),
        P("tp", None),
    )
    out_specs = P(("sp", "tp"), None)
    run = functools.partial(body, mesh.shape["sp"], mesh.shape["tp"])
    return jax.shard_map(run, mesh=mesh, in_specs=in_specs, out_specs=out_specs, check_vma=False)
```

time: 317 us -> 87.7 us (0.28)
  blocking collectives: 132 us -> 0 us
  Pallas kernels: 0 us -> 72.9 us
  waiting for transfers between devices: 68.7 us -> 0 us
  matrix products: 39.2 us -> 0 us
  local copies, waits for them, and re-layouts: 43 us -> 3.93 us
  between operations: 13.6 us -> 0.03 us
  other arithmetic: 18.8 us -> 10.4 us
    all_gather x3 -> x0, blocking collectives: 129 us -> none  [the longest x1 45 us: body(): lax.all_gather(values, 'sp', axis=0, tiled=True)]
    pallas_call x0 -> x1, Pallas kernels: none -> 72.9 us  [body(): pl.pallas_call(functools.partial(kernel, (S, T, G, R, B, Cr, cw)), out_sh...]
    all_gather x3 -> x0, waiting for transfers between devices: 61.5 us -> none  [the longest x1 56.5 us: body(): lax.all_gather(latent_keys, 'sp', axis=0, tiled=True)]
    dot_general x30 -> x0, matrix products: 39.2 us -> none  [the longest x10 12.1 us: update(): jnp.einsum('hqk,khe->qhe', exp_weights.astype(jnp.bfloat16), values_heads...]
    dynamic_slice x16 -> x0, local copies, waits for them, and re-layouts: 33.9 us -> none  [fold_keys(): carry, unused = lax.scan(update, carry, blocks)]
    reduce_sum x8 -> x0, other arithmetic: 11 us -> none  [the longest x5 8.09 us: update(): totals = totals * rescale + jnp.sum(exp_weights, axis=-1)]
    gather x0 -> x1, other arithmetic: none -> 9.86 us  [rotation_tables(): rate = rates[lane % quarter]]
    reduce_scatter x1 -> x0, waiting for transfers between devices: 7.15 us -> none  [body(): lax.psum_scatter(jnp.dot(heads_out, output_weight, preferred_element_type...]
  transfers between devices with their start and end apart: 4 -> 0, of which waited for: 3 -> 0; matrix products, arithmetic and copies ran while one was open for 6% -> 0% of each run, Pallas kernels for 0% -> 0%
where the time goes in v1:
time: 87.7 us; the launch traced here: 87.3 us
  Pallas kernels  72.9 us (83%)
  other arithmetic  10.4 us (12%)
  local copies, waits for them, and re-layouts  3.93 us (4%)
    pallas_call x1, Pallas kernels, body(): pl.pallas_call(functools.partial(kernel, (S, T, G, R, B, Cr, cw)), out_sh...  72.9 us
    gather x1, other arithmetic, rotation_tables(): rate = rates[lane % quarter]  9.86 us
    unnamed x1, local copies, waits for them, and re-layouts  1.88 us

profile of v1, /device:TPU:0, one launch (start us, length us, event | category | flops | bytes accessed | tf_op | source)
XLA Modules:
  0.0 87.3 jit_solution(16168883643457816764)
XLA Ops:
  0.0 0.7 fusion.5
  0.7 9.9 %bitcast_select_fusion.8 = (f32[128]{0:T(128)S(1)}, f32[128]{0:T(128)S(1)}) fusion(f32[]{:T(128)} %bitcast.21, f32[]{:T(128)} %bitcast.22, f32[]{:T(128)} %bitcast.23, f32[]{:T(128)} %bitcast.24, f32[]{:T(128)} %bitcast.25, f32[]{:T(128)} %bitcast.27, f32[]{:T(128)} %bitcast.26, f32[]{:T(128)} %bitcast.4, f32[]{:T(128)} %bitcast.6, f32[]{:T(128)} %bitcast.8, ...), kind=kLoop, calls=%fused_computation.16 | loop fusion | flops 8832 | bytes 1088 | tf_op jit(solution)/shard_map/gather | solution.py:29
  10.6 0.6 sine_multiply_fusion
  11.2 0.7 concatenate.7.sin_ref
  11.8 0.7 concatenate.6.cos_ref
  12.5 72.9 %shard_map.136 = bf16[128,2048]{1,0:T(8,128)(2,1)} custom-call(bf16[128,2048]{1,0:T(8,128)(2,1)} %latent_ref.1, bf16[32,2048]{1,0:T(8,128)(2,1)} %context_ref.1, f32[1,1024]{1,0:T(1,128)} %bitcast.57, f32[1,1024]{1,0:T(1,128)} %bitcast.58, bf16[1024,384]{1,0:T(8,128)(2,1)} %modw_ref.1, bf16[2048,256]{1,0:T(8,128)(2,1)} %wq1_hbm.1, ...), custom_call_target="tpu_custom_call" | custom-call | tf_op jit(solution)/shard_map/pallas_call | solution.py:356
  85.4 1.9 %copy.16 = bf16[128,2048]{1,0:T(8,128)(2,1)} copy(bf16[128,2048]{1,0:T(8,128)(2,1)} %shard_map.136) | data formatting | bytes 1048576
  (3 shorter events, 0.0 us)

commit v2 on v1

--- a/solution.py
+++ b/solution.py
@@ -3,6 +3,7 @@
 
 import jax
 import jax.numpy as jnp
+import numpy as np
 from jax import lax
 from jax.experimental import pallas as pl
 from jax.experimental.pallas import tpu as pltpu
@@ -19,22 +20,21 @@
 BF16 = jnp.bfloat16
 F32 = jnp.float32
 LANES = 128
-
-
-def rotation_tables(positions, extra):
+QROWS = 256
+
+
+def rotation_tables(grid_rows):
     half = HEAD_DIM // 2
     quarter = half // 2
-    rates = THETA ** (-jnp.arange(quarter, dtype=F32) / quarter)
-    lane = jnp.arange(LANES) % HEAD_DIM
-    rate = rates[lane % quarter]
-    where = jnp.where(
-        (lane < half)[None, :], (positions // GRID_W)[:, None], (positions % GRID_W)[:, None]
-    ).astype(F32)
-    angle = where * rate[None, :]
-    sign = jnp.where(lane % half < quarter, -1.0, 1.0).astype(F32)
-    cosine = jnp.concatenate([jnp.cos(angle), jnp.ones((extra, LANES), F32)], 0)
-    sine = jnp.concatenate([jnp.sin(angle) * sign[None, :], jnp.zeros((extra, LANES), F32)], 0)
-    return cosine, sine
+    lane = np.arange(LANES) % HEAD_DIM
+    rate = (THETA ** (-(lane % quarter) / quarter)).astype(np.float32)
+    sign = np.where(lane % half < quarter, -1.0, 1.0)
+    tables = []
+    for count, mask in ((grid_rows, lane < half), (GRID_W, lane >= half)):
+        angle = np.arange(count, dtype=np.float32)[:, None] * rate[None, :]
+        for table in (np.cos(angle), np.sin(angle) * sign):
+            tables.append(np.where(mask, table, 0.0).astype(np.float32))
+    return tables
 
 
 def rotate(x, cosine, sine):
@@ -46,21 +46,20 @@
     return x * cosine + flipped * sine
 
 
-def normed_rows(rows, scale, shift):
+def normed_rows(rows):
     v = rows.astype(F32)
-    v = v * lax.rsqrt(jnp.mean(v * v, axis=-1, keepdims=True) + EPSILON)
-    return (v * (1.0 + scale) + shift).astype(BF16)
+    return v * lax.rsqrt(jnp.mean(v * v, axis=-1, keepdims=True) + EPSILON)
 
 
 def kernel(
     dims,
     latent_ref, context_ref, cond_ref, ccond_ref, modw_ref,
     wq1_hbm, wq2_hbm, wk1_hbm, wk2_hbm, wv_hbm,
-    lam_ref, boost_ref, gain_ref, wo_hbm, cos_ref, sin_ref,
+    lam_ref, boost_ref, gain_ref, wo_hbm, crow_ref, srow_ref, ccol_ref, scol_ref,
     out_ref,
     wq1, wq2, wk1, wk2, wv, wo,
-    sig, modp, modall, modrow, lat, h,
-    qs, kvs, q, kv, mx, den, acc, ho, hr, rsend, rs,
+    cos_ref, sin_ref, sig, modp, modall, modrow, lat, nrm, h,
+    qs, kvs, q, kv, mx, acc, ho, hr, rsend, rs,
     wsem, mp_s, mp_r, lt_s, lt_r, ma_s, ma_r,
     q_s, q_r, kz_s, kv_s, kv_r, ho_s, ho_r, rs_s, rs_r,
 ):
@@ -80,7 +79,7 @@
     loads = [
         pltpu.make_async_copy(a, b, wsem.at[i])
         for i, (a, b) in enumerate(
-            [(wk1_hbm, wk1), (wk2_hbm, wk2), (wv_hbm, wv), (wq1_hbm, wq1), (wq2_hbm, wq2), (wo_hbm, wo)]
+            [(wq1_hbm, wq1), (wq2_hbm, wq2), (wk1_hbm, wk1), (wk2_hbm, wk2), (wv_hbm, wv), (wo_hbm, wo)]
         )
     ]
     for load in loads:
@@ -95,6 +94,13 @@
     for i in range(1, T):
         pl.semaphore_signal(barrier, inc=1, device_id=(s, (t + i) % T), device_id_type=MESH)
 
+    for i in range(Lr // GRID_W):
+        span, at = slice(i * GRID_W, (i + 1) * GRID_W), pl.ds(s * (Lr // GRID_W) + i, 1)
+        cos_ref[span, :] = ccol_ref[...] + crow_ref[at, :]
+        sin_ref[span, :] = scol_ref[...] + srow_ref[at, :]
+    cos_ref[Lr:, :] = jnp.ones((Cp, LANES), F32)
+    sin_ref[Lr:, :] = jnp.zeros((Cp, LANES), F32)
+
     for i, ref in enumerate((cond_ref, ccond_ref)):
         v = ref[...]
         sig[i : i + 1, :] = v / (1.0 + jnp.exp(-v))
@@ -131,6 +137,15 @@
     for i in range(1, T):
         o = (t + i) % T
         remote(lat.at[o], lat.at[o], lt_s.at[i], lt_r.at[o], s, o).wait_recv()
+    step = math.gcd(rows, 32)
+    for i in range(T):
+
+        @pl.loop(0, rows // step)
+        def _(j):
+            at = pl.multiple_of(j * step, step)
+            nrm[pl.ds(i * rows + at, step), :] = normed_rows(lat[i, pl.ds(at, step), :])
+
+    nrm[Lr:, :] = normed_rows(context_ref[...])
 
     @pl.loop(1, S)
     def _(i):
@@ -139,19 +154,33 @@
     for i in range(S):
         modrow[:, i * cw : (i + 1) * cw] = modall[i][:, :cw]
 
-    step = math.gcd(rows, 32)
-    for i in range(T):
-
-        @pl.loop(0, rows // step)
-        def _(j):
-            at = pl.multiple_of(j * step, step)
-            h[pl.ds(i * rows + at, step), :] = normed_rows(
-                lat[i, pl.ds(at, step), :], modrow[0:1, D : 2 * D], modrow[0:1, :D]
-            )
-
-    h[Lr:, :] = normed_rows(context_ref[...], modrow[1:2, D : 2 * D], modrow[1:2, :D])
-
-    for i in range(3):
+    @pl.loop(0, Lr // step)
+    def _(j):
+        at = pl.ds(pl.multiple_of(j * step, step), step)
+        h[at, :] = (nrm[at, :] * (1.0 + modrow[0:1, D : 2 * D]) + modrow[0:1, :D]).astype(BF16)
+
+    h[Lr:, :] = (nrm[Lr:, :] * (1.0 + modrow[1:2, D : 2 * D]) + modrow[1:2, :D]).astype(BF16)
+
+    for i in range(2):
+        loads[i].wait()
+    lh = h[:Lr, :]
+    one = jnp.dot(lh, wq1[...], preferred_element_type=F32)
+    two = jnp.dot(lh, wq2[...], preferred_element_type=F32)
+    for i in range(G):
+        cut = slice(i * HEAD_DIM, (i + 1) * HEAD_DIM)
+        pair = jnp.concatenate([one[:, cut], two[:, cut]], axis=1)
+        turned = rotate(pair, cos_ref[:Lr, :], sin_ref[:Lr, :])
+        qs[i] = (turned * (LOG2E * HEAD_DIM**-0.5)).astype(BF16)
+
+    def q_out(i):
+        to = (g + i) % G
+        return remote(qs.at[to], q.at[g], q_s.at[i], q_r.at[g], to * R + r, t)
+
+    for i in range(1, G):
+        q_out(i).start()
+    q[g] = qs[g]
+
+    for i in range(2, 5):
         loads[i].wait()
     hh = h[...]
     one = jnp.dot(hh, wk1[...], preferred_element_type=F32)
@@ -185,27 +214,7 @@
             forward(i, j).start()
 
     forward_all(0)
-    for i in range(3, 5):
-        loads[i].wait()
-    lh = h[:Lr, :]
-    one = jnp.dot(lh, wq1[...], preferred_element_type=F32)
-    two = jnp.dot(lh, wq2[...], preferred_element_type=F32)
-    for i in range(G):
-        cut = slice(i * HEAD_DIM, (i + 1) * HEAD_DIM)
-        pair = jnp.concatenate([one[:, cut], two[:, cut]], axis=1)
-        turned = rotate(pair, cos_ref[:Lr, :], sin_ref[:Lr, :])
-        qs[i] = (turned * (LOG2E * HEAD_DIM**-0.5)).astype(BF16)
-
-    def q_out(i):
-        to = (g + i) % G
-        return remote(qs.at[to], q.at[g], q_s.at[i], q_r.at[g], to * R + r, t)
-
-    for i in range(1, G):
-        q_out(i).start()
-    q[g] = qs[g]
-
     mx[...] = jnp.full(mx.shape, NEGATIVE, F32)
-    den[...] = jnp.zeros(den.shape, F32)
     acc[...] = jnp.zeros(acc.shape, F32)
     boost = boost_ref[g] * LOG2E
 
@@ -213,72 +222,97 @@
         o = (g + i) % G
         remote(q.at[o], q.at[o], q_s.at[i], q_r.at[o], s, t).wait_recv()
 
+    def attend(n, at):
+        k_l = kv[pl.ds(at, B), :Lr, :LANES].reshape(B * Lr, LANES)
+        v_l = kv[pl.ds(at, B), :Lr, LANES:].reshape(B * Lr, VALUE_DIM)
+        k_c = kv[pl.ds(at, B), Lr:, :LANES].reshape(B * Cp, LANES)
+        v_c = kv[pl.ds(at, B), Lr:, LANES:].reshape(B * Cp, VALUE_DIM)
+        v_l = jnp.concatenate([v_l, jnp.ones_like(v_l)], axis=1)
+        v_c = jnp.concatenate([v_c, jnp.ones_like(v_c)], axis=1)
+        nt = (((1,), (1,)), ((), ()))
+        QB = min(Lr, QROWS)
+        for m, c in [(m, c) for c in range(Lr // QB) for m in range(2)]:
+            part = slice(c * QB, (c + 1) * QB)
+            qq = q[n, part, :]
+            lane = lax.broadcasted_iota(jnp.int32, qq.shape, 1)
+            qm = jnp.where(lane // HEAD_DIM == m, qq, jnp.zeros_like(qq))
+            s_l = lax.dot_general(qm, k_l, nt, preferred_element_type=F32)
+            s_c = lax.dot_general(qm, k_c, nt, preferred_element_type=F32) + boost
+            if Cp != Cr:
+                spot = lax.broadcasted_iota(jnp.int32, s_c.shape, 1)
+                s_c = jnp.where(spot % Cp < Cr, s_c, NEGATIVE)
+            old = mx[m, n, part, :]
+            peak = jnp.maximum(
+                old,
+                jnp.maximum(
+                    jnp.max(s_l, axis=-1, keepdims=True), jnp.max(s_c, axis=-1, keepdims=True)
+                ),
+            )
+            p_l = jnp.exp2(s_l - peak).astype(BF16)
+            p_c = jnp.exp2(s_c - peak).astype(BF16)
+            mx[m, n, part, :] = peak
+            acc[m, n, part, :] = (
+                jnp.exp2(old - peak) * acc[m, n, part, :]
+                + jnp.dot(p_l, v_l, preferred_element_type=F32)
+                + jnp.dot(p_c, v_c, preferred_element_type=F32)
+            )
+
+    lam = lam_ref[g]
+    gain = gain_ref[...]
+
+    def finish(n):
+        one = acc[0, n, :, :VALUE_DIM] / acc[0, n, :, VALUE_DIM:]
+        two = acc[1, n, :, :VALUE_DIM] / acc[1, n, :, VALUE_DIM:]
+        mixed = one - lam * two
+        mixed = mixed * lax.rsqrt(jnp.mean(mixed * mixed, axis=-1, keepdims=True) + EPSILON) * gain
+        return mixed.astype(BF16)
+
+    def ho_out(i):
+        to = (g + i) % G
+        return remote(ho.at[to], hr.at[g], ho_s.at[i], ho_r.at[g], to * R + r, t)
+
+    def pass_on(i):
+        landed(((g + G - i) % G) * R + r)
+        forward_all(i)
+
     for i in range(G):
-        if i + 1 < G:
-            landed(((g + G - i - 1) % G) * R + r)
-            forward_all(i + 1)
+        if i == 1 and G > 2:
+            pass_on(2)
         base = ((g + G - i) % G) * R
 
         @pl.loop(1, R)
         def _(j):
             landed(base + (r + j) % R)
 
-        @pl.loop(0, (R // B) * G)
-        def _(n):
-            at = base + (n // G) * B
-            n = n % G
-            k_l = kv[pl.ds(at, B), :Lr, :LANES].reshape(B * Lr, LANES)
-            v_l = kv[pl.ds(at, B), :Lr, LANES:].reshape(B * Lr, VALUE_DIM)
-            k_c = kv[pl.ds(at, B), Lr:, :LANES].reshape(B * Cp, LANES)
-            v_c = kv[pl.ds(at, B), Lr:, LANES:].reshape(B * Cp, VALUE_DIM)
-            qq = q[n]
-            lane = lax.broadcasted_iota(jnp.int32, qq.shape, 1)
-            nt = (((1,), (1,)), ((), ()))
-            for m in range(2):
-                qm = jnp.where(lane // HEAD_DIM == m, qq, jnp.zeros_like(qq))
-                s_l = lax.dot_general(qm, k_l, nt, preferred_element_type=F32)
-                s_c = lax.dot_general(qm, k_c, nt, preferred_element_type=F32) + boost
-                if Cp != Cr:
-                    spot = lax.broadcasted_iota(jnp.int32, s_c.shape, 1)
-                    s_c = jnp.where(spot % Cp < Cr, s_c, NEGATIVE)
-                old = mx[m, n]
-                peak = jnp.maximum(
-                    old,
-                    jnp.maximum(
-                        jnp.max(s_l, axis=-1, keepdims=True), jnp.max(s_c, axis=-1, keepdims=True)
-                    ),
-                )
-                p_l = jnp.exp2(s_l - peak)
-                p_c = jnp.exp2(s_c - peak)
-                alpha = jnp.exp2(old - peak)
-                mx[m, n] = peak
-                den[m, n] = (
-                    alpha * den[m, n]
-                    + jnp.sum(p_l, axis=-1, keepdims=True)
-                    + jnp.sum(p_c, axis=-1, keepdims=True)
-                )
-                acc[m, n] = (
-                    alpha * acc[m, n]
-                    + jnp.dot(p_l.astype(BF16), v_l, preferred_element_type=F32)
-                    + jnp.dot(p_c.astype(BF16), v_c, preferred_element_type=F32)
-                )
-
-    lam = lam_ref[g]
-    gain = gain_ref[...]
-
-    def ho_out(i):
-        to = (g + i) % G
-        return remote(ho.at[to], hr.at[g], ho_s.at[i], ho_r.at[g], to * R + r, t)
-
-    for i in range(1, G + 1):
-        n = (g + i) % G
-        mixed = acc[0, n] / den[0, n] - lam * (acc[1, n] / den[1, n])
-        mixed = mixed * lax.rsqrt(jnp.mean(mixed * mixed, axis=-1, keepdims=True) + EPSILON) * gain
-        if i < G:
-            ho[n] = mixed.astype(BF16)
-            ho_out(i).start()
+        if i + 1 < G:
+            half = G // 2
+            for low, high in ((0, half), (half, G)):
+                if low and i == 0:
+                    pass_on(1)
+                elif low and i + 2 < G:
+                    pass_on(i + 2)
+
+                @pl.loop(low * (R // B), high * (R // B))
+                def _(x):
+                    attend(x // (R // B), base + x % (R // B) * B)
+
         else:
-            hr[g] = mixed.astype(BF16)
+
+            @pl.loop(1, G + 1)
+            def _(y):
+                n = (g + y) % G
+
+                @pl.loop(0, R // B)
+                def _(x):
+                    attend(n, base + x * B)
+
+                ho[n] = finish(n)
+
+                @pl.when(y < G)
+                def _():
+                    ho_out(y).start()
+
+    hr[g] = ho[g]
     loads[5].wait()
     for i in range(1, G):
         o = (g + i) % G
@@ -345,8 +379,8 @@
     if cp != cw:
         modulation_weight = jnp.pad(modulation_weight, ((0, 0), (0, cp - cw)))
     depth = modulation_weight.shape[0]
-    positions = lax.axis_index("sp") * Lr + jnp.arange(Lr, dtype=jnp.int32)
-    cosine, sine = rotation_tables(positions, Cp)
+    assert Lr % GRID_W == 0
+    tables = rotation_tables(S * Lr // GRID_W)
     vm = pl.BlockSpec(memory_space=pltpu.VMEM)
     sm = pl.BlockSpec(memory_space=pltpu.SMEM)
     hb = pl.BlockSpec(memory_space=pl.ANY)
@@ -356,23 +390,25 @@
     return pl.pallas_call(
         functools.partial(kernel, (S, T, G, R, B, Cr, cw)),
         out_shape=jax.ShapeDtypeStruct((rows, D), BF16),
-        in_specs=[vm] * 5 + [hb] * 5 + [sm, sm, vm, hb, vm, vm],
+        in_specs=[vm] * 5 + [hb] * 5 + [sm, sm, vm, hb, vm, vm, vm, vm],
         out_specs=vm,
         scratch_shapes=[V(w.shape, BF16) for w in weights]
         + [
+            V((Lr + Cp, LANES), F32),
+            V((Lr + Cp, LANES), F32),
             V((2, depth), F32),
             V((T, 2, cp), F32),
             V((S, 2, cp), F32),
             V((2, 3 * D), F32),
             V((T, rows, D), BF16),
+            V((Lr + Cp, D), F32),
             V((Lr + Cp, D), BF16),
             V((G, Lr, LANES), BF16),
             V((G, Lr + Cp, LANES + VALUE_DIM), BF16),
             V((G, Lr, LANES), BF16),
             V((S, Lr + Cp, LANES + VALUE_DIM), BF16),
             V((2, G, Lr, 1), F32),
-            V((2, G, Lr, 1), F32),
-            V((2, G, Lr, VALUE_DIM), F32),
+            V((2, G, Lr, 2 * VALUE_DIM), F32),
             V((G, Lr, VALUE_DIM), BF16),
             V((G, Lr, VALUE_DIM), BF16),
             V((T, rows, D), BF16),
@@ -388,7 +424,7 @@
     )(
         latent, context, condition[None, :], context_condition[None, :], modulation_weight,
         query_first, query_second, key_first, key_second, value_weight,
-        lambda_head, context_score_boost, head_gain[None, :], output_weight, cosine, sine,
+        lambda_head, context_score_boost, head_gain[None, :], output_weight, *tables,
     )
 
 

time: 87.7 us -> 64.8 us (0.74)
  Pallas kernels: 72.9 us -> 62.3 us
  other arithmetic: 10.4 us -> 0 us
  local copies, waits for them, and re-layouts: 3.93 us -> 1.88 us
    pallas_call x1, Pallas kernels: 72.9 us -> 62.3 us  [body(): pl.pallas_call(functools.partial(kernel, (S, T, G, R, B, Cr, cw)), out_sh...]
    gather x1 -> x0, other arithmetic: 9.86 us -> none  [rotation_tables(): rate = rates[lane % quarter]]
    concatenate x2 -> x0, local copies, waits for them, and re-layouts: 1.33 us -> none  [the longest x1 0.67 us: rotation_tables(): cosine = jnp.concatenate([jnp.cos(angle), jnp.ones((extra, LANES), F32)], 0)]
where the time goes in v2:
time: 64.8 us; the launch traced here: 64.2 us
  Pallas kernels  62.3 us (96%)
  local copies, waits for them, and re-layouts  1.88 us (3%)
    pallas_call x1, Pallas kernels, body(): pl.pallas_call(functools.partial(kernel, (S, T, G, R, B, Cr, cw)), out_sh...  62.3 us
    unnamed x1, local copies, waits for them, and re-layouts  1.88 us

profile of v2, /device:TPU:0, one launch (start us, length us, event | category | flops | bytes accessed | tf_op | source)
XLA Modules:
  0.0 64.2 jit_solution(16930760007500322690)
XLA Ops:
  0.0 62.3 %shard_map.172 = bf16[128,2048]{1,0:T(8,128)(2,1)} custom-call(bf16[128,2048]{1,0:T(8,128)(2,1)} %latent_ref.1, bf16[32,2048]{1,0:T(8,128)(2,1)} %context_ref.1, f32[1,1024]{1,0:T(1,128)} %bitcast.3, f32[1,1024]{1,0:T(1,128)} %bitcast.4, bf16[1024,384]{1,0:T(8,128)(2,1)} %modw_ref.1, bf16[2048,256]{1,0:T(8,128)(2,1)} %wq1_hbm.1, bf16[2048,256]{1,0:T(8,128)(2,1)} %wq2_hbm.1, ...), custom_call_target="tpu_custom_call" | custom-call | tf_op jit(solution)/shard_map/pallas_call | solution.py:390
  62.3 1.9 %copy.20 = bf16[128,2048]{1,0:T(8,128)(2,1)} copy(bf16[128,2048]{1,0:T(8,128)(2,1)} %shard_map.172) | data formatting | bytes 1048576
